TPU v7x, 32 devices: a whole 2x2x4 slice. The times are simulated.
32 devices in a mesh: grp: 2 (over y), sp: 4 (over z), tp: 4 (over x, core).
Axes of the slice: x: 2, y: 2, z: 4, core: 2. Of those that a mesh axis runs over, the one named last changes fastest.
Arguments:
- queries: bfloat16 [4096, 1024], P(('grp', 'sp'), 'tp'), parts along dimension 0, may hold values from -6 to 6
- memory_keys: bfloat16 [4096, 1024], P(('grp', 'sp'), 'tp'), parts along dimension 0, may hold values from -6 to 6
- memory_values: bfloat16 [4096, 1024], P(('grp', 'sp'), 'tp'), parts along dimension 0, may hold values from -6 to 6
- output_preactivation: bfloat16 [4096, 1024], P(('grp', 'sp'), 'tp'), parts along dimension 0, may hold values from -12 to 12
- input_preactivation: float32 [8, 4096], P('tp', ('grp', 'sp')), parts along dimension 1, may hold values from -6 to 140
- forget_preactivation: float32 [8, 4096], P('tp', ('grp', 'sp')), parts along dimension 1, as said below
- extra_forget_terms: float32 [8, 4096], P('tp', ('grp', 'sp')), parts along dimension 1, may hold values from -1 to 0, as said below
- head_norm_gain: float32 [128], replicated, may hold values from 0.1 to 1.9
- output_projection_matrix: bfloat16 [1024, 2048], P('tp'), may hold values from -0.1875 to 0.1875
- residual: bfloat16 [4096, 2048], P(('grp', 'sp', 'tp')), parts along dimension 0, may hold values from -6 to 6
- feedforward_norm_gain: float32 [2048], replicated, may hold values from 0.1 to 1.9
- feedforward_up_matrix: bfloat16 [2048, 8192], P('sp', 'tp'), may hold values from -0.125 to 0.125
- feedforward_down_matrix: bfloat16 [8192, 2048], P('tp', 'sp'), may hold values from -0.0625 to 0.0625
Outputs:
- layer_out: bfloat16 [4096, 2048], P(('grp', 'sp', 'tp')), parts along dimension 0
There are 2 independent parts, one for each index of `grp`. A program takes and returns all parts, laid end to end along the dimension named above; an argument that names none is the same for every part. Nothing has to cross between parts.
Inputs may be any that keep to these rules, and one draw needn't show every extreme that they name: `forget_preactivation`: forget gate pre-activations. `extra_forget_terms`: extra log forget terms, zero at most positions.
All inputs are finite; a program needn't handle non-finite values.
Results may differ from a plain program's by a relative error of at most 0.018.
Values may be sent and summed in bfloat16 or wider, within the bound.
A program may use at most 64 MiB of HBM per device.

v0:
```python
import jax
import jax.numpy as jnp
from jax import lax
from jax.sharding import PartitionSpec as P

BLOCK = 128


neg_big = -1e30
norm_eps = 1e-06
highest = lax.Precision.HIGHEST


def entering(x, axis, combine, identity):
    length, position = (lax.axis_size(axis), lax.axis_index(axis))
    everything = jax.tree.map(lambda part: lax.all_gather(part, axis), x)
    start = jax.tree.map(
        lambda part, zero: jnp.broadcast_to(jnp.asarray(zero, part.dtype), part.shape), x, identity
    )

    def step(k, before):
        reached = k < position
        new = combine(before, jax.tree.map(lambda part: part[k], everything))
        return jax.tree.map(lambda a, b: jnp.where(reached, a, b), new, before)

    return lax.fori_loop(0, length, step, start)


def rms_norm(tensor, gain_vec):
    mean_sq = jnp.mean(tensor * tensor, axis=-1, keepdims=True)
    return tensor * lax.rsqrt(mean_sq + norm_eps) * gain_vec


def combine(earlier, later):
    total_e, max_e, memory_e = earlier
    total_l, max_l, memory_l = later
    carried = total_l + max_e
    new_max = jnp.maximum(carried, max_l)
    old_part = jnp.exp(carried - new_max)
    new_part = jnp.exp(max_l - new_max)
    return (
        total_e + total_l,
        new_max,
        old_part[..., None, None] * memory_e + new_part[..., None, None] * memory_l,
    )


def block_summary(key_blk, val_blk, gate_blk, decay_logarithm):
    block_total = decay_logarithm[..., -1]
    tail_log = block_total[..., None] - decay_logarithm + gate_blk
    tail_max = jnp.max(tail_log, axis=-1)
    weights = jnp.exp(tail_log - tail_max[..., None])
    memory = jnp.einsum("bhsv,bhsk->bhvk", weights[..., None] * val_blk, key_blk, precision=highest)
    return (block_total, tail_max, memory)


def shards(
    queries,
    memory_keys,
    memory_values,
    output_preactivation,
    input_preactivation,
    forget_preactivation,
    extra_forget_terms,
    head_norm_gain,
    output_projection_matrix,
    residual,
    feedforward_norm_gain,
    feedforward_up_matrix,
    feedforward_down_matrix,
):
    tok_count = queries.shape[0]
    head_count = input_preactivation.shape[0]
    head_dim = queries.shape[1] // head_count
    block_len = BLOCK
    block_count = tok_count // block_len

    def to_blocks(tensor):
        return (
            tensor.astype(jnp.float32)
            .reshape(block_count, block_len, head_count, head_dim)
            .transpose(0, 2, 1, 3)
        )

    def gate_block_list(tensor):
        return tensor.reshape(head_count, block_count, block_len).transpose(1, 0, 2)

    query_blk = to_blocks(queries)
    key_blk = to_blocks(memory_keys) * head_dim ** (-0.5)
    val_blk = to_blocks(memory_values)
    gate_blk = gate_block_list(input_preactivation)
    decay_logarithm = jnp.cumsum(
        gate_block_list(jax.nn.log_sigmoid(forget_preactivation) + extra_forget_terms), axis=-1
    )
    summaries = block_summary(key_blk, val_blk, gate_blk, decay_logarithm)
    zero_heads = jnp.zeros((head_count,), jnp.float32)
    zero_memory = jnp.zeros((head_count, head_dim, head_dim), jnp.float32)
    zero_state = (zero_heads, jnp.full((head_count,), neg_big, jnp.float32), zero_memory)
    prefixes = []
    running = zero_state
    for block_idx in range(block_count):
        prefixes.append(running)
        running = combine(running, tuple((member[block_idx] for member in summaries)))
    before = entering(running, "sp", combine, zero_state)
    anchor = (zero_heads, zero_heads, zero_memory)
    incoming = combine(anchor, before)
    starts = [combine(incoming, prefix) for prefix in prefixes]
    start_max = jnp.stack([each_state[1] for each_state in starts])
    start_memory = jnp.stack([each_state[2] for each_state in starts])
    causal = lax.broadcasted_iota(jnp.int32, (block_len, block_len), 0) >= lax.broadcasted_iota(
        jnp.int32, (block_len, block_len), 1
    )
    log_weight = (
        decay_logarithm[..., :, None] - decay_logarithm[..., None, :] + gate_blk[..., None, :]
    )
    log_weight = jnp.where(causal, log_weight, neg_big)
    carry_log = decay_logarithm + start_max[..., None]
    row_max = jnp.maximum(jnp.max(log_weight, axis=-1), carry_log)
    scores = jnp.einsum("bhtd,bhsd->bhts", query_blk, key_blk, precision=highest) * jnp.exp(
        log_weight - row_max[..., None]
    )
    carry_scale = jnp.exp(carry_log - row_max)
    hidden = jnp.einsum("bhts,bhsv->bhtv", scores, val_blk, precision=highest)
    hidden = hidden + carry_scale[..., None] * jnp.einsum(
        "bhvk,bhtk->bhtv", start_memory, query_blk, precision=highest
    )
    hidden = hidden.transpose(0, 2, 1, 3).reshape(tok_count, head_count, head_dim)
    gated = rms_norm(hidden, head_norm_gain) * jax.nn.sigmoid(
        output_preactivation.astype(jnp.float32).reshape(tok_count, head_count, head_dim)
    )
    mixed = gated.reshape(tok_count, head_count * head_dim).astype(jnp.bfloat16)
    branch = lax.psum_scatter(
        jnp.dot(mixed, output_projection_matrix, preferred_element_type=jnp.float32).astype(
            jnp.bfloat16
        ),
        "tp",
        scatter_dimension=0,
        tiled=True,
    ).astype(jnp.float32)
    mid_state = (residual.astype(jnp.float32) + branch).astype(jnp.bfloat16)
    normed = rms_norm(mid_state.astype(jnp.float32), feedforward_norm_gain).astype(jnp.bfloat16)
    normed_all = lax.all_gather(normed, "tp", axis=0, tiled=True)
    upward = jnp.dot(
        normed_all,
        lax.all_gather(feedforward_up_matrix, "sp", axis=0, tiled=True),
        preferred_element_type=jnp.float32,
    )
    active = jnp.square(jax.nn.relu(upward)).astype(jnp.bfloat16)
    mlp_terms = jnp.dot(
        active,
        lax.all_gather(feedforward_down_matrix, "sp", axis=1, tiled=True),
        preferred_element_type=jnp.float32,
    )
    mlp_sum = lax.psum_scatter(
        mlp_terms.astype(jnp.bfloat16), "tp", scatter_dimension=0, tiled=True
    ).astype(jnp.float32)
    return (mid_state.astype(jnp.float32) + mlp_sum).astype(jnp.bfloat16)


def solution(mesh):
    in_specs = (
        P(("grp", "sp"), "tp"),
        P(("grp", "sp"), "tp"),
        P(("grp", "sp"), "tp"),
        P(("grp", "sp"), "tp"),
        P("tp", ("grp", "sp")),
        P("tp", ("grp", "sp")),
        P("tp", ("grp", "sp")),
        P(),
        P("tp", None),
        P(("grp", "sp", "tp"), None),
        P(),
        P("sp", "tp"),
        P("tp", "sp"),
    )
    out_specs = P(("grp", "sp", "tp"), None)
    return jax.shard_map(shards, mesh=mesh, in_specs=in_specs, out_specs=out_specs, check_vma=False)
```

profile of v0, /device:TPU:24, one launch (start us, length us, event | category | flops | bytes accessed | tf_op | source)
XLA Modules:
  0.0 467.1 jit_solution(10719103995341335332)
XLA Ops:
  6.5 0.0 copy-start
  6.5 0.0 reduce-scatter.3.cloned.1.call-start
  6.6 0.8 fusion.50
  7.4 1.2 reduce_window_sum.11
  8.7 0.2 slice_reduce_fusion.3
  8.9 0.1 slice.64
  8.9 0.1 copy.51
  9.0 0.1 copy.52
  9.1 0.9 fusion.65
  10.0 0.8 subtract_exponential_fusion.2
  10.8 7.3 %all-gather.1 = f32[4,1,2]{2,1,0:T(1,128)S(1)} all-gather(f32[1,1,2]{2,1,0:T(1,128)S(1)} %get-tuple-element.255), channel_id=1, replica_groups=mesh['grp'=2,'sp'=4,'tp'=4] {'sp'}, dimensions={0}, use_global_device_ids=true | all-gather | bytes 40 | tf_op jit(solution)/shard_map/all_gather | solution.py:16
  18.2 9.8 %all-gather = f32[4,1,2]{2,1,0:T(1,128)S(1)} all-gather(f32[1,1,2]{2,1,0:T(1,128)S(1)} %get-tuple-element.256), channel_id=1, replica_groups=mesh['grp'=2,'sp'=4,'tp'=4] {'sp'}, dimensions={0}, use_global_device_ids=true | all-gather | bytes 40 | tf_op jit(solution)/shard_map/all_gather | solution.py:16
  28.0 1.0 reshape.306
  29.0 0.2 copy.54
  29.2 1.0 convert_multiply_fusion.2
  30.2 0.3 mul.301
  30.5 0.7 fusion.22
  31.2 0.1 fusion.40
  31.3 15.7 %all_gather.23 = f32[4,2,128,128]{3,2,1,0:T(8,128)S(1)} all-gather(f32[1,2,128,128]{3,2,1,0:T(8,128)S(1)} %fusion.40), channel_id=1, replica_groups=mesh['grp'=2,'sp'=4,'tp'=4] {'sp'}, dimensions={0}, use_global_device_ids=true | all-gather | bytes 655360 | tf_op jit(solution)/shard_map/all_gather | solution.py:16
  47.0 0.6 while.18
  47.0 0.1 fusion.73
  47.2 0.1 fusion.73
  47.3 0.1 fusion.73
  47.5 0.1 fusion.73
  47.7 0.0 copy-done.4
  47.7 0.3 fusion.27
  48.0 0.1 fusion.47
  48.1 0.1 add_maximum_fusion
  48.2 0.0 copy-done.7
  48.2 0.0 copy-done.3
  48.2 0.1 reshape.303
  48.3 0.0 copy-start.6
  48.3 0.7 fusion.5
  49.0 0.1 add_bitcast_fusion
  49.2 0.1 add_bitcast_fusion.2
  49.3 0.7 fusion.7
  49.9 0.4 multiply_reduce_fusion
  50.4 0.2 copy.59
  50.6 0.0 copy-start.1
  50.6 0.3 copy.58
  50.8 0.6 mul.356
  51.4 0.0 copy-start.5
  51.5 0.0 copy-done
  51.5 0.0 copy-done.6
  51.5 2.1 convolution_convert_fusion
  53.6 0.0 reduce-scatter.3.cloned.1.call-update
  53.6 0.0 all-gather.6.cloned.1.call-start
  53.7 32.2 %reduce-scatter.3.cloned.1.call-done = bf16[128,2048]{1,0:T(8,128)(2,1)} async-done(((bf16[512,2048]{1,0:T(8,128)(2,1)}), bf16[128,2048]{1,0:T(8,128)(2,1)}) %reduce-scatter.3.cloned.1.call-update) | async-done | bytes 524304 | tf_op jit(solution)/shard_map/reduce_scatter | solution.py:132
  85.9 1.3 fusion.8
  87.2 2.0 fusion.10
  89.2 0.0 all-gather.6.cloned.1.call-update
  89.3 0.0 all-gather.8.cloned.1.call-start
  89.3 0.7 all-gather.8.cloned.1.call-update
  90.0 0.0 all-gather.10.cloned.1.call-start
  90.1 0.5 all-gather.10.cloned.1.call-update
  90.6 0.0 copy-start.2
  90.6 0.2 reduce-scatter.5.cloned.1.call-start
  90.8 21.2 %all-gather.6.cloned.1.call-done = bf16[512,2048]{1,0:T(8,128)(2,1)} async-done(((bf16[128,2048]{1,0:T(8,128)(2,1)}), bf16[512,2048]{1,0:T(8,128)(2,1)}) %all-gather.6.cloned.1.call-update) | async-done | bytes 2097168 | tf_op jit(solution)/shard_map/all_gather | solution.py:142
  112.0 148.2 %all-gather.8.cloned.1.call-done = bf16[2048,2048]{1,0:T(8,128)(2,1)} async-done(((bf16[512,2048]{1,0:T(8,128)(2,1)}), bf16[2048,2048]{1,0:T(8,128)(2,1)}) %all-gather.8.cloned.1.call-update) | async-done | bytes 8388624 | tf_op jit(solution)/shard_map/all_gather | solution.py:145
  260.2 149.3 %all-gather.10.cloned.1.call-done = bf16[2048,2048]{1,0:T(8,128)(2,1)} async-done(((bf16[2048,512]{1,0:T(8,128)(2,1)}), bf16[2048,2048]{1,0:T(8,128)(2,1)}) %all-gather.10.cloned.1.call-update) | async-done | bytes 8388624 | tf_op jit(solution)/shard_map/all_gather | solution.py:151
  409.4 16.5 %convolution_convert_fusion.1 = bf16[512,2048]{1,0:T(8,128)(2,1)} fusion(bf16[2048,2048]{1,0:T(8,128)(2,1)} %all-gather.10.cloned.1.call-done, bf16[512,2048]{1,0:T(8,128)(2,1)} %all-gather.6.cloned.1.call-done, bf16[2048,2048]{1,0:T(8,128)(2,1)} %all-gather.8.cloned.1.call-done), kind=kOutput, calls=%fused_computation.16 | convolution fusion | flops 8594128896 | bytes 20971520 | tf_op jit(solution)/shard_map/dot_general | solution.py:149
  426.0 0.0 reduce-scatter.5.cloned.1.call-update
  426.0 32.6 %reduce-scatter.5.cloned.1.call-done = bf16[128,2048]{1,0:T(8,128)(2,1)} async-done(((bf16[512,2048]{1,0:T(8,128)(2,1)}), bf16[128,2048]{1,0:T(8,128)(2,1)}) %reduce-scatter.5.cloned.1.call-update) | async-done | bytes 524304 | tf_op jit(solution)/shard_map/reduce_scatter | solution.py:154
  458.5 2.1 fusion.11
  (28 shorter events, 0.3 us)
Async XLA Ops:
  6.5 44.9 %copy-start = (bf16[256,2048]{1,0:T(8,128)(2,1)S(1)}, bf16[256,2048]{1,0:T(8,128)(2,1)}, u32[]{:S(2)}) copy-start(bf16[256,2048]{1,0:T(8,128)(2,1)} %param.23) | copy-start | bytes 3145732
  6.5 41.1 %copy-start.4 = (f32[2,512]{1,0:T(2,128)S(1)}, f32[2,512]{1,0:T(2,128)}, u32[]{:S(2)}) copy-start(f32[2,512]{1,0:T(2,128)} %param.19) | copy-start | bytes 12292
  6.5 41.7 %copy-start.7 = (f32[128]{0:T(128)S(1)}, f32[128]{0:T(128)}, u32[]{:S(2)}) copy-start(f32[128]{0:T(128)} %param.22) | copy-start | bytes 1540
  6.5 41.7 %copy-start.3 = (bf16[512,256]{1,0:T(8,128)(2,1)S(1)}, bf16[512,256]{1,0:T(8,128)(2,1)}, u32[]{:S(2)}) copy-start(bf16[512,256]{1,0:T(8,128)(2,1)} %param.15) | copy-start | bytes 786436
  6.5 79.3 %reduce-scatter.3.cloned.1.call-start = ((), (), s32[]{:S(2)}) async-start(), calls=%async_computation.2 | async-start | bytes 2621440 | tf_op jit(solution)/shard_map/reduce_scatter | solution.py:132
  48.3 3.2 copy-start.6
  50.6 35.3 %copy-start.1 = (bf16[128,2048]{1,0:T(8,128)(2,1)S(1)}, bf16[128,2048]{1,0:T(8,128)(2,1)}, u32[]{:S(2)}) copy-start(bf16[128,2048]{1,0:T(8,128)(2,1)} %param.24) | copy-start | bytes 1572868
  51.4 35.8 %copy-start.5 = (f32[2048]{0:T(1024)S(1)}, f32[2048]{0:T(1024)}, u32[]{:S(2)}) copy-start(f32[2048]{0:T(1024)} %param.25) | copy-start | bytes 24580
  53.6 58.4 %all-gather.6.cloned.1.call-start = ((), (), s32[]{:S(2)}) async-start(), calls=%async_computation.3 | async-start | bytes 2621440 | tf_op jit(solution)/shard_map/all_gather | solution.py:142
  89.3 170.9 %all-gather.8.cloned.1.call-start = ((), (), s32[]{:S(2)}) async-start(), calls=%async_computation.4 | async-start | bytes 10485760 | tf_op jit(solution)/shard_map/all_gather | solution.py:145
  90.0 319.4 %all-gather.10.cloned.1.call-start = ((), (), s32[]{:S(2)}) async-start(), calls=%async_computation.5 | async-start | bytes 10485760 | tf_op jit(solution)/shard_map/all_gather | solution.py:151
  90.6 368.0 %copy-start.2 = (bf16[128,2048]{1,0:T(8,128)(2,1)S(1)}, bf16[128,2048]{1,0:T(8,128)(2,1)}, u32[]{:S(2)}) copy-start(bf16[128,2048]{1,0:T(8,128)(2,1)} %reduce-scatter.3.cloned.1.call-done) | copy-start | bytes 1572868
  90.6 367.9 %reduce-scatter.5.cloned.1.call-start = ((), (), s32[]{:S(2)}) async-start(), calls=%async_computation.6 | async-start | bytes 2621440 | tf_op jit(solution)/shard_map/reduce_scatter | solution.py:154
Sparse Core Ops, SparseCore 0:
  53.7 32.1 reduce-scatter.2
  89.4 22.5 all-gather.5
  113.6 146.5 all-gather.7
  261.6 147.7 all-gather.9
  426.1 32.3 reduce-scatter.4
where the time goes:
time: 469 us; the launch traced here: 467 us
  waiting for transfers between devices  385 us (82%)
  blocking collectives  32.8 us (7%)
  matrix products  21.1 us (4%)
  between operations  13.4 us (3%)
  other arithmetic  11.6 us (2%)
    all_gather x1, waiting for transfers between devices, shards(): lax.all_gather(feedforward_down_matrix, 'sp', axis=1, tiled=True)  149 us
    all_gather x1, waiting for transfers between devices, shards(): lax.all_gather(feedforward_up_matrix, 'sp', axis=0, tiled=True)  148 us
    all_gather x3, blocking collectives, entering(): everything = jax.tree.map(lambda part: lax.all_gather(part, axis), x)  32.8 us
    reduce_scatter x1, waiting for transfers between devices, shards(): lax.psum_scatter(mlp_terms.astype(jnp.bfloat16), 'tp', scatter_dimension=...  32.6 us
    reduce_scatter x1, waiting for transfers between devices, shards(): lax.psum_scatter(jnp.dot(mixed, output_projection_matrix, preferred_eleme...  32.2 us
    all_gather x1, waiting for transfers between devices, shards(): normed_all = lax.all_gather(normed, 'tp', axis=0, tiled=True)  21.2 us
    dot_general x1, matrix products, shards(): jnp.dot(active, lax.all_gather(feedforward_down_matrix, 'sp', axis=1, til...  16.5 us
  transfers between devices with their start and end apart: 5, of which 5 were waited for; matrix products, arithmetic and copies ran while one was open for 0% of the time, Pallas kernels for 0%

commit v1 on v0

v1 whole, which is shorter than its diff:
```python
import functools

import jax
import jax.numpy as jnp
from jax import lax
from jax.experimental import pallas as pl
from jax.experimental.pallas import tpu as pltpu
from jax.sharding import PartitionSpec as P

BLOCK = 128
EPS = 1e-06
NEG = -1e30
MESH = pl.DeviceIdType.MESH
F32 = jnp.float32
BF16 = jnp.bfloat16


def split_dot(exact, wide, swap=False):
    high = wide.astype(BF16)
    low = (wide - high.astype(F32)).astype(BF16)
    if swap:
        return jnp.dot(high, exact, preferred_element_type=F32) + jnp.dot(
            low, exact, preferred_element_type=F32
        )
    return jnp.dot(exact, high, preferred_element_type=F32) + jnp.dot(
        exact, low, preferred_element_type=F32
    )


def kernel(
    dims,
    q_ref, k_ref, v_ref, o_ref, arow_ref, acol_ref, ccol_ref, hgain_ref, wout_ref, res_ref,
    fgain_ref, up_ref, down_ref,
    mid_ref, mlp_ref,
    upw, dnw, ntok, act, msend, mrecv, bsend, brecv, mixed, blockmem, st_out, st_in,
    w_send, w_recv, loc_sem, st_send, st_recv, b_send, b_recv, t_send, t_recv, f_send, m_send, m_recv,
):
    grp, sp, tp, heads, blocks, rows = dims
    g, z, t = lax.axis_index("grp"), lax.axis_index("sp"), lax.axis_index("tp")
    layer = grp * tp
    me = g * tp + t
    half = tp // 2
    chunks = upw.shape[1]

    def there(gg, zz, tt):
        return {"grp": gg, "sp": zz, "tp": tt}

    barrier = pltpu.get_barrier_semaphore()
    for j in range(1, layer):
        d = lax.rem(me + j, layer)
        pl.semaphore_signal(
            barrier, inc=1, device_id=there(d // tp, z, lax.rem(d, tp)), device_id_type=MESH
        )

    @pl.when(z > 0)
    def _():
        pl.semaphore_signal(barrier, inc=1, device_id=there(g, z - 1, t), device_id_type=MESH)

    @pl.when(z < sp - 1)
    def _():
        pl.semaphore_signal(barrier, inc=1, device_id=there(g, z + 1, t), device_id_type=MESH)

    neighbours = (z + sp - 1) // sp + (2 * sp - 2 - z) // sp
    pl.semaphore_wait(barrier, layer - 1 + neighbours)

    hidden_half = up_ref.shape[1] // grp
    bufs = (upw, dnw)

    def own_piece(m, c):
        n = bufs[m].shape[2]
        if m == 0:
            return up_ref.at[
                pl.ds(c * n, n), pl.ds(pl.multiple_of(g * hidden_half, 128), hidden_half)
            ]
        return down_ref.at[pl.ds(pl.multiple_of(g * hidden_half + c * n, 16), n), :]

    def weight_copy(m, c, origin, way, source=None):
        dst = bufs[m].at[origin, c]
        zz = z + 1 if way == 0 else z - 1
        return pltpu.make_async_remote_copy(
            src_ref=dst if source is None else source,
            dst_ref=dst,
            send_sem=w_send.at[m, way, origin, c],
            recv_sem=w_recv.at[m, origin, c],
            device_id=there(g, zz, t),
            device_id_type=MESH,
        )

    def local_copy(m, c):
        return pltpu.make_async_copy(own_piece(m, c), bufs[m].at[z, c], loc_sem.at[m, c])

    def start_own(m):
        for c in range(chunks):
            @pl.when(z < sp - 1)
            def _():
                weight_copy(m, c, z, 0, own_piece(m, c)).start()

            @pl.when(z > 0)
            def _():
                weight_copy(m, c, z, 1, own_piece(m, c)).start()

    def relay(m, s):
        left, right = z - 1 - s, z + 1 + s
        for c in range(chunks):
            @pl.when(left >= 0)
            def _():
                weight_copy(m, c, left, 0).wait_recv()

                @pl.when(z < sp - 1)
                def _():
                    weight_copy(m, c, left, 0).start()

            @pl.when(right < sp)
            def _():
                weight_copy(m, c, right, 1).wait_recv()

                @pl.when(z > 0)
                def _():
                    weight_copy(m, c, right, 1).start()

    def relays(m, first, last):
        def body(s, _):
            relay(m, s)
            return 0

        lax.fori_loop(first, last, body, 0)

    start_own(0)
    for m in range(2):
        for c in range(chunks):
            local_copy(m, c).start()

    scale = BLOCK ** (-0.5) if q_ref.shape[1] // heads == BLOCK else (q_ref.shape[1] // heads) ** (-0.5)
    dh = q_ref.shape[1] // heads
    totals, tails = {}, {}
    for h in range(heads):
        cols = pl.ds(h * dh, dh)
        run = None
        for b in range(blocks):
            at = pl.ds(b * BLOCK, BLOCK)
            cum = ccol_ref[at, h : h + 1]
            total = cum[BLOCK - 1 : BLOCK, :]
            tail = total + acol_ref[at, h : h + 1]
            tail_max = jnp.max(tail, axis=0, keepdims=True)
            weighted = v_ref[at, cols].astype(F32) * jnp.exp(tail - tail_max)
            key_t = k_ref[at, cols].astype(F32).T.astype(BF16)
            mem = split_dot(key_t, weighted) * scale
            blockmem[h, b] = mem
            totals[h, b], tails[h, b] = total, tail_max
            if run is None:
                run = (total, tail_max, mem)
            else:
                new = jnp.maximum(total + run[1], tail_max)
                run = (
                    total + run[0],
                    new,
                    jnp.exp(total + run[1] - new) * run[2] + jnp.exp(tail_max - new) * mem,
                )
        st_out[h, :dh, :] = run[2]
        st_out[h, dh : dh + 8, :] = jnp.broadcast_to(run[1], (8, dh))
        st_out[h, dh + 8 : dh + 16, :] = jnp.broadcast_to(run[0], (8, dh))

    def state_copy():
        return pltpu.make_async_remote_copy(
            src_ref=st_out,
            dst_ref=st_in,
            send_sem=st_send,
            recv_sem=st_recv,
            device_id=there(g, z + 1, t),
            device_id_type=MESH,
        )

    @pl.when(z == 0)
    def _():
        st_in[...] = jnp.zeros_like(st_in)

    @pl.when(z > 0)
    def _():
        state_copy().wait_recv()

    @pl.when(z < sp - 1)
    def _():
        for h in range(heads):
            m_in = st_in[h, dh : dh + 1, :]
            m_loc = st_out[h, dh : dh + 1, :]
            total = st_out[h, dh + 8 : dh + 9, :]
            new = jnp.maximum(total + m_in, m_loc)
            st_out[h, :dh, :] = (
                jnp.exp(total + m_in - new) * st_in[h, :dh, :]
                + jnp.exp(m_loc - new) * st_out[h, :dh, :]
            )
            st_out[h, dh : dh + 8, :] = jnp.broadcast_to(new, (8, dh))
        state_copy().start()

    third = (sp - 1) // 3
    relays(0, 0, third)

    causal = lax.broadcasted_iota(jnp.int32, (BLOCK, BLOCK), 0) >= lax.broadcasted_iota(
        jnp.int32, (BLOCK, BLOCK), 1
    )
    gain = hgain_ref[...]
    for h in range(heads):
        cols = pl.ds(h * dh, dh)
        memory = st_in[h, :dh, :]
        stab = st_in[h, dh : dh + 1, 0:1]
        for b in range(blocks):
            at = pl.ds(b * BLOCK, BLOCK)
            cum = ccol_ref[at, h : h + 1]
            query = q_ref[at, cols]
            key_t = k_ref[at, cols].astype(F32).T.astype(BF16)
            log_weight = jnp.where(causal, cum + arow_ref[h * blocks + b : h * blocks + b + 1, :], NEG)
            carry = cum + stab
            row_max = jnp.maximum(jnp.max(log_weight, axis=1, keepdims=True), carry)
            scores = (
                jnp.dot(query, key_t, preferred_element_type=F32)
                * scale
                * jnp.exp(log_weight - row_max)
            )
            hidden = split_dot(v_ref[at, cols], scores, swap=True)
            hidden = hidden + jnp.exp(carry - row_max) * split_dot(query, memory)
            mean_sq = jnp.mean(hidden * hidden, axis=1, keepdims=True)
            gate = o_ref[at, cols].astype(F32)
            out = hidden * lax.rsqrt(mean_sq + EPS) * gain * (1.0 / (1.0 + jnp.exp(-gate)))
            mixed[at, cols] = out.astype(BF16)
            total, tail_max = totals[h, b], tails[h, b]
            new = jnp.maximum(total + stab, tail_max)
            memory = jnp.exp(total + stab - new) * memory + jnp.exp(tail_max - new) * blockmem[h, b]
            stab = new

    def branch_copy(j):
        d = lax.rem(t + j, tp)
        return pltpu.make_async_remote_copy(
            src_ref=bsend.at[j],
            dst_ref=brecv.at[j],
            send_sem=b_send.at[j],
            recv_sem=b_recv.at[j],
            device_id=there(g, z, d),
            device_id_type=MESH,
        )

    for j in list(range(1, tp)) + [0]:
        d = lax.rem(t + j, tp)
        part = jnp.dot(
            mixed[pl.ds(pl.multiple_of(d * rows, rows), rows), :],
            wout_ref[...],
            preferred_element_type=F32,
        )
        bsend[j] = part.astype(BF16)
        if j:
            branch_copy(j).start()

    branch = bsend[0].astype(F32)
    for j in range(1, tp):
        branch_copy(j).wait_recv()
        branch = branch + brecv[j].astype(F32)
    mid = (res_ref[...].astype(F32) + branch).astype(BF16)
    mid_ref[...] = mid
    wide = mid.astype(F32)
    mean_sq = jnp.mean(wide * wide, axis=1, keepdims=True)
    ntok[me] = (wide * lax.rsqrt(mean_sq + EPS) * fgain_ref[...]).astype(BF16)

    place = g * half + t // 2
    core = lax.rem(t, 2)
    same = grp * half

    def peer(j):
        there_at = lax.rem(place + j, same)
        return there_at // half, lax.rem(there_at, half) * 2 + core

    def token_copy(j, back=False):
        gg, tt = peer(j)
        slot = (gg * tp + tt) if back else me
        return pltpu.make_async_remote_copy(
            src_ref=ntok.at[slot],
            dst_ref=ntok.at[slot],
            send_sem=t_send.at[j],
            recv_sem=t_recv.at[slot],
            device_id=there(gg, z, tt),
            device_id_type=MESH,
        )

    def partner_copy(j, mine=True):
        gg, tt = peer(j)
        slot = gg * tp + (tt if mine else tt + 1 - 2 * core)
        return pltpu.make_async_remote_copy(
            src_ref=ntok.at[slot],
            dst_ref=ntok.at[slot],
            send_sem=f_send.at[j],
            recv_sem=t_recv.at[slot],
            device_id=there(g, z, t + 1 - 2 * core),
            device_id_type=MESH,
        )

    for j in range(1, same):
        token_copy(j).start()
    partner_copy(0).start()
    relays(0, third, 2 * third)
    start_own(1)
    for j in range(1, same):
        token_copy(j, back=True).wait_recv()
        partner_copy(j).start()
    for j in range(same):
        partner_copy(j, mine=False).wait_recv()
    relays(0, 2 * third, sp - 1)
    for m in range(2):
        for c in range(chunks):
            local_copy(m, c).wait()

    width = ntok.shape[2]
    pack = 2

    def up_step(i, _):
        x = ntok[pl.ds(i * pack, pack)].reshape(pack * rows, width)
        y = jnp.dot(x, upw[...].reshape(width, hidden_half), preferred_element_type=F32)
        y = jnp.maximum(y, 0.0)
        act[pl.ds(i * pack, pack)] = (y * y).astype(BF16).reshape(pack, rows, hidden_half)
        return 0

    lax.fori_loop(0, layer // pack, up_step, 0)

    out_cols = down_ref.shape[1]

    def mlp_copy(origin, j):
        d = lax.rem(me + j, layer)
        return pltpu.make_async_remote_copy(
            src_ref=msend.at[origin, j],
            dst_ref=mrecv.at[origin, j],
            send_sem=m_send.at[origin, j],
            recv_sem=m_recv.at[origin, j],
            device_id=there(d // tp, z, lax.rem(d, tp)),
            device_id_type=MESH,
        )

    def down_piece(origin):
        w = dnw[origin].reshape(hidden_half, out_cols)

        def step(i, _):
            j = layer - 1 - i
            x = act[lax.rem(me + j, layer)]
            msend[origin, j] = jnp.dot(x, w, preferred_element_type=F32).astype(BF16)

            @pl.when(j > 0)
            def _():
                mlp_copy(origin, j).start()

            return 0

        lax.fori_loop(0, layer, step, 0)

    down_piece(z)

    def down_step(s, _):
        relay(1, s)

        @pl.when(z - 1 - s >= 0)
        def _():
            down_piece(z - 1 - s)

        @pl.when(z + 1 + s < sp)
        def _():
            down_piece(z + 1 + s)

        return 0

    lax.fori_loop(0, sp - 1, down_step, 0)

    def finish(origin, _):
        total = msend[origin, 0].astype(F32)
        for j in range(1, layer):
            mlp_copy(origin, j).wait_recv()
            total = total + mrecv[origin, j].astype(F32)
        mlp_ref[origin] = total
        return 0

    lax.fori_loop(0, sp, finish, 0)

    def drain(origin, _):
        for j in range(1, layer):
            mlp_copy(origin, j).wait_send()
        for m in range(2):
            for c in range(chunks):
                @pl.when((origin <= z) & (z < sp - 1))
                def _():
                    weight_copy(m, c, origin, 0).wait_send()

                @pl.when((origin >= z) & (z > 0))
                def _():
                    weight_copy(m, c, origin, 1).wait_send()
        return 0

    lax.fori_loop(0, sp, drain, 0)
    for j in range(1, tp):
        branch_copy(j).wait_send()
    for j in range(1, same):
        token_copy(j).wait_send()
    for j in range(same):
        partner_copy(j).wait_send()

    @pl.when(z < sp - 1)
    def _():
        state_copy().wait_send()


def shards(
    mesh_shape,
    queries, memory_keys, memory_values, output_preactivation, input_preactivation,
    forget_preactivation, extra_forget_terms, head_norm_gain, output_projection_matrix, residual,
    feedforward_norm_gain, feedforward_up_matrix, feedforward_down_matrix,
):
    grp, sp, tp = mesh_shape
    tokens = queries.shape[0]
    heads = input_preactivation.shape[0]
    blocks = tokens // BLOCK
    dh = queries.shape[1] // heads
    rows, width = residual.shape
    layer = grp * tp
    up_rows, hidden = feedforward_up_matrix.shape
    hidden_half = hidden // grp
    out_cols = feedforward_down_matrix.shape[1]
    chunks = 2

    log_forget = jax.nn.log_sigmoid(forget_preactivation) + extra_forget_terms
    cum = jnp.cumsum(log_forget.reshape(heads, blocks, BLOCK), axis=-1)
    rest = input_preactivation.reshape(heads, blocks, BLOCK) - cum
    arow = rest.reshape(heads * blocks, BLOCK)
    acol = rest.reshape(heads, tokens).T
    ccol = cum.reshape(heads, tokens).T

    vmem = pl.BlockSpec(memory_space=pltpu.VMEM)
    hbm = pl.BlockSpec(memory_space=pl.ANY)
    dma = pltpu.SemaphoreType.DMA
    mid, mlp = pl.pallas_call(
        functools.partial(kernel, (grp, sp, tp, heads, blocks, rows)),
        out_shape=(
            jax.ShapeDtypeStruct((rows, width), BF16),
            jax.ShapeDtypeStruct((sp, rows, out_cols), F32),
        ),
        in_specs=[vmem] * 11 + [hbm] * 2,
        out_specs=(vmem, vmem),
        scratch_shapes=[
            pltpu.VMEM((sp, chunks, up_rows // chunks, hidden_half), BF16),
            pltpu.VMEM((sp, chunks, hidden_half // chunks, out_cols), BF16),
            pltpu.VMEM((layer, rows, width), BF16),
            pltpu.VMEM((layer, rows, hidden_half), BF16),
            pltpu.VMEM((sp, layer, rows, out_cols), BF16),
            pltpu.VMEM((sp, layer, rows, out_cols), BF16),
            pltpu.VMEM((tp, rows, width), BF16),
            pltpu.VMEM((tp, rows, width), BF16),
            pltpu.VMEM((tokens, heads * dh), BF16),
            pltpu.VMEM((heads, blocks, dh, dh), F32),
            pltpu.VMEM((heads, dh + 16, dh), F32),
            pltpu.VMEM((heads, dh + 16, dh), F32),
            dma((2, 2, sp, chunks)),
            dma((2, sp, chunks)),
            dma((2, chunks)),
            dma,
            dma,
            dma((tp,)),
            dma((tp,)),
            dma((layer,)),
            dma((layer,)),
            dma((layer,)),
            dma((sp, layer)),
            dma((sp, layer)),
        ],
        compiler_params=pltpu.CompilerParams(
            collective_id=0, has_side_effects=True, vmem_limit_bytes=60 * 1024 * 1024
        ),
    )(
        queries, memory_keys, memory_values, output_preactivation, arow, acol, ccol,
        head_norm_gain.reshape(1, dh), output_projection_matrix, residual,
        feedforward_norm_gain.reshape(1, width), feedforward_up_matrix, feedforward_down_matrix,
    )
    mlp = mlp.transpose(1, 0, 2).reshape(rows, width)
    return (mid.astype(F32) + mlp).astype(BF16)


def solution(mesh):
    in_specs = (
        P(("grp", "sp"), "tp"),
        P(("grp", "sp"), "tp"),
        P(("grp", "sp"), "tp"),
        P(("grp", "sp"), "tp"),
        P("tp", ("grp", "sp")),
        P("tp", ("grp", "sp")),
        P("tp", ("grp", "sp")),
        P(),
        P("tp", None),
        P(("grp", "sp", "tp"), None),
        P(),
        P("sp", "tp"),
        P("tp", "sp"),
    )
    out_specs = P(("grp", "sp", "tp"), None)
    shape = (mesh.shape["grp"], mesh.shape["sp"], mesh.shape["tp"])
    return jax.shard_map(
        functools.partial(shards, shape),
        mesh=mesh,
        in_specs=in_specs,
        out_specs=out_specs,
        check_vma=False,
    )
```

time: 469 us -> 176 us (0.38)
  waiting for transfers between devices: 385 us -> 0 us
  Pallas kernels: 0 us -> 168 us
  blocking collectives: 32.8 us -> 0 us
  matrix products: 21.1 us -> 0 us
  between operations: 13.4 us -> 0.07 us
  other arithmetic: 11.6 us -> 3.57 us
    all_gather x3 -> x0, waiting for transfers between devices: 319 us -> none  [the longest x1 149 us: shards(): lax.all_gather(feedforward_down_matrix, 'sp', axis=1, tiled=True)]
    pallas_call x0 -> x1, Pallas kernels: none -> 168 us  [shards(): pl.pallas_call(functools.partial(kernel, (grp, sp, tp, heads, blocks, row...]
    reduce_scatter x2 -> x0, waiting for transfers between devices: 64.8 us -> none  [the longest x1 32.6 us: shards(): lax.psum_scatter(mlp_terms.astype(jnp.bfloat16), 'tp', scatter_dimension=...]
    all_gather x3 -> x0, blocking collectives: 32.8 us -> none  [entering(): everything = jax.tree.map(lambda part: lax.all_gather(part, axis), x)]
    dot_general x6 -> x0, matrix products: 21.1 us -> none  [the longest x1 16.5 us: shards(): jnp.dot(active, lax.all_gather(feedforward_down_matrix, 'sp', axis=1, til...]
  transfers between devices with their start and end apart: 5 -> 0, of which waited for: 5 -> 0; matrix products, arithmetic and copies ran while one was open for 0% -> 0% of each run, Pallas kernels for 0% -> 0%
where the time goes in v1:
time: 176 us
  Pallas kernels  168 us (95%)
  local copies, waits for them, and re-layouts  3.65 us (2%)
  other arithmetic  3.57 us (2%)
    pallas_call x1, Pallas kernels, shards(): pl.pallas_call(functools.partial(kernel, (grp, sp, tp, heads, blocks, row...  168 us

profile of v1, /device:TPU:24, one launch (start us, length us, event | category | flops | bytes accessed | tf_op | source)
XLA Modules:
  0.0 175.7 jit_solution(5737383450284935493)
XLA Ops:
  0.0 0.7 fusion.1
  0.7 0.6 reduce_window_sum.15
  1.4 0.7 reshape.21
  2.1 0.6 sub.7.arow_ref
  2.7 0.1 copy.16
  2.8 0.0 copy-start
  2.8 0.9 copy.17
  3.7 0.7 bitcast_subtract_fusion
  4.4 0.0 copy-done
  4.4 168.4 %shard_map.127 = (bf16[128,2048]{1,0:T(8,128)(2,1)}, f32[4,128,512]{2,1,0:T(8,128)}) custom-call(bf16[512,256]{1,0:T(8,128)(2,1)} %q_ref.1, bf16[512,256]{1,0:T(8,128)(2,1)} %k_ref.1, bf16[512,256]{1,0:T(8,128)(2,1)} %v_ref.1, bf16[512,256]{1,0:T(8,128)(2,1)} %o_ref.1, f32[8,128]{1,0:T(8,128)} %sub.7.arow_ref, f32[512,2]{1,0:T(8,128)} %bitcast.12, ...), custom_call_target="tpu_custom_call" | custom-call | tf_op jit(solution)/shard_map/pallas_call | solution.py:432
  172.8 0.0 copy-start.1
  172.8 1.6 copy.18
  174.5 0.3 copy.19
  174.8 0.0 copy-done.1
  174.8 0.9 add_convert_fusion
  (1 shorter events, 0.0 us)
Async XLA Ops:
  2.8 1.6 copy-start
  172.8 2.0 %copy-start.1 = (bf16[128,2048]{1,0:T(8,128)(2,1)S(1)}, bf16[128,2048]{1,0:T(8,128)(2,1)}, u32[]{:S(2)}) copy-start(bf16[128,2048]{1,0:T(8,128)(2,1)} %get-tuple-element.7) | copy-start | bytes 1572868

commit v2 on v1

--- a/solution.py
+++ b/solution.py
@@ -32,15 +32,22 @@
     q_ref, k_ref, v_ref, o_ref, arow_ref, acol_ref, ccol_ref, hgain_ref, wout_ref, res_ref,
     fgain_ref, up_ref, down_ref,
     mid_ref, mlp_ref,
-    upw, dnw, ntok, act, msend, mrecv, bsend, brecv, mixed, blockmem, st_out, st_in,
-    w_send, w_recv, loc_sem, st_send, st_recv, b_send, b_recv, t_send, t_recv, f_send, m_send, m_recv,
+    upw, dnw, ntok, act, psend, precv, msend, mrecv, cbuf, crecv, bsend, brecv, mixed, blockmem, st_out, st_in,
+    w_send, w_recv, loc_sem, st_send, st_recv, c_send, c_recv, b_send, b_recv, t_send, t_recv, f_send,
+    p_send, p_recv, m_send, m_recv,
 ):
     grp, sp, tp, heads, blocks, rows = dims
     g, z, t = lax.axis_index("grp"), lax.axis_index("sp"), lax.axis_index("tp")
     layer = grp * tp
     me = g * tp + t
     half = tp // 2
-    chunks = upw.shape[1]
+    same = grp * half
+    core = lax.rem(t, 2)
+    pair = t // 2
+    place = g * half + pair
+    mine = core * same + place
+    partner = t + 1 - 2 * core
+    counts = (upw.shape[1], dnw.shape[1])
 
     def there(gg, zz, tt):
         return {"grp": gg, "sp": zz, "tp": tt}
@@ -72,7 +79,10 @@
             return up_ref.at[
                 pl.ds(c * n, n), pl.ds(pl.multiple_of(g * hidden_half, 128), hidden_half)
             ]
-        return down_ref.at[pl.ds(pl.multiple_of(g * hidden_half + c * n, 16), n), :]
+        n = bufs[m].shape[3]
+        return down_ref.at[
+            pl.ds(pl.multiple_of(g * hidden_half, 16), hidden_half), pl.ds(c * n, n)
+        ]
 
     def weight_copy(m, c, origin, way, source=None):
         dst = bufs[m].at[origin, c]
@@ -90,7 +100,7 @@
         return pltpu.make_async_copy(own_piece(m, c), bufs[m].at[z, c], loc_sem.at[m, c])
 
     def start_own(m):
-        for c in range(chunks):
+        for c in range(counts[m]):
             @pl.when(z < sp - 1)
             def _():
                 weight_copy(m, c, z, 0, own_piece(m, c)).start()
@@ -99,35 +109,36 @@
             def _():
                 weight_copy(m, c, z, 1, own_piece(m, c)).start()
 
-    def relay(m, s):
+    def relay(m, s, c):
         left, right = z - 1 - s, z + 1 + s
-        for c in range(chunks):
-            @pl.when(left >= 0)
-            def _():
-                weight_copy(m, c, left, 0).wait_recv()
-
-                @pl.when(z < sp - 1)
-                def _():
-                    weight_copy(m, c, left, 0).start()
-
-            @pl.when(right < sp)
-            def _():
-                weight_copy(m, c, right, 1).wait_recv()
-
-                @pl.when(z > 0)
-                def _():
-                    weight_copy(m, c, right, 1).start()
-
-    def relays(m, first, last):
+
+        @pl.when(left >= 0)
+        def _():
+            weight_copy(m, c, left, 0).wait_recv()
+
+            @pl.when(z < sp - 1)
+            def _():
+                weight_copy(m, c, left, 0).start()
+
+        @pl.when(right < sp)
+        def _():
+            weight_copy(m, c, right, 1).wait_recv()
+
+            @pl.when(z > 0)
+            def _():
+                weight_copy(m, c, right, 1).start()
+
+    def relays(first, last):
         def body(s, _):
-            relay(m, s)
+            for c in range(counts[0]):
+                relay(0, s, c)
             return 0
 
         lax.fori_loop(first, last, body, 0)
 
     start_own(0)
     for m in range(2):
-        for c in range(chunks):
+        for c in range(counts[m]):
             local_copy(m, c).start()
 
     scale = BLOCK ** (-0.5) if q_ref.shape[1] // heads == BLOCK else (q_ref.shape[1] // heads) ** (-0.5)
@@ -193,7 +204,7 @@
         state_copy().start()
 
     third = (sp - 1) // 3
-    relays(0, 0, third)
+    relays(0, third)
 
     causal = lax.broadcasted_iota(jnp.int32, (BLOCK, BLOCK), 0) >= lax.broadcasted_iota(
         jnp.int32, (BLOCK, BLOCK), 1
@@ -227,158 +238,209 @@
             memory = jnp.exp(total + stab - new) * memory + jnp.exp(tail_max - new) * blockmem[h, b]
             stab = new
 
-    def branch_copy(j):
-        d = lax.rem(t + j, tp)
-        return pltpu.make_async_remote_copy(
-            src_ref=bsend.at[j],
-            dst_ref=brecv.at[j],
-            send_sem=b_send.at[j],
-            recv_sem=b_recv.at[j],
-            device_id=there(g, z, d),
-            device_id_type=MESH,
-        )
-
-    for j in list(range(1, tp)) + [0]:
-        d = lax.rem(t + j, tp)
-        part = jnp.dot(
+    def cross_copy(q):
+        return pltpu.make_async_remote_copy(
+            src_ref=cbuf.at[q],
+            dst_ref=crecv.at[q],
+            send_sem=c_send.at[q],
+            recv_sem=c_recv.at[q],
+            device_id=there(g, z, partner),
+            device_id_type=MESH,
+        )
+
+    def branch_copy(q, slot):
+        return pltpu.make_async_remote_copy(
+            src_ref=bsend.at[q],
+            dst_ref=brecv.at[slot],
+            send_sem=b_send.at[q],
+            recv_sem=b_recv.at[slot],
+            device_id=there(g, z, 2 * q + core),
+            device_id_type=MESH,
+        )
+
+    def branch_part(d):
+        return jnp.dot(
             mixed[pl.ds(pl.multiple_of(d * rows, rows), rows), :],
             wout_ref[...],
             preferred_element_type=F32,
         )
-        bsend[j] = part.astype(BF16)
-        if j:
-            branch_copy(j).start()
-
-    branch = bsend[0].astype(F32)
-    for j in range(1, tp):
-        branch_copy(j).wait_recv()
-        branch = branch + brecv[j].astype(F32)
-    mid = (res_ref[...].astype(F32) + branch).astype(BF16)
+
+    for q in range(half):
+        cbuf[q] = branch_part(2 * q + 1 - core).astype(BF16)
+        cross_copy(q).start()
+    for q in range(half):
+        part = branch_part(2 * q + core)
+        cross_copy(q).wait_recv()
+        bsend[q] = (part + crecv[q].astype(F32)).astype(BF16)
+
+        @pl.when(q != pair)
+        def _():
+            branch_copy(q, pair).start()
+
+    brecv[pair] = bsend[pair]
+    branch = res_ref[...].astype(F32)
+    for q in range(half):
+        @pl.when(q != pair)
+        def _():
+            branch_copy(q, q).wait_recv()
+
+        branch = branch + brecv[q].astype(F32)
+    mid = branch.astype(BF16)
     mid_ref[...] = mid
     wide = mid.astype(F32)
     mean_sq = jnp.mean(wide * wide, axis=1, keepdims=True)
-    ntok[me] = (wide * lax.rsqrt(mean_sq + EPS) * fgain_ref[...]).astype(BF16)
-
-    place = g * half + t // 2
-    core = lax.rem(t, 2)
-    same = grp * half
-
-    def peer(j):
-        there_at = lax.rem(place + j, same)
-        return there_at // half, lax.rem(there_at, half) * 2 + core
-
-    def token_copy(j, back=False):
-        gg, tt = peer(j)
-        slot = (gg * tp + tt) if back else me
+    ntok[mine] = (wide * lax.rsqrt(mean_sq + EPS) * fgain_ref[...]).astype(BF16)
+
+    def token_copy(j, slot):
+        at = lax.rem(place + j, same)
         return pltpu.make_async_remote_copy(
             src_ref=ntok.at[slot],
             dst_ref=ntok.at[slot],
             send_sem=t_send.at[j],
             recv_sem=t_recv.at[slot],
-            device_id=there(gg, z, tt),
-            device_id_type=MESH,
-        )
-
-    def partner_copy(j, mine=True):
-        gg, tt = peer(j)
-        slot = gg * tp + (tt if mine else tt + 1 - 2 * core)
+            device_id=there(at // half, z, lax.rem(at, half) * 2 + core),
+            device_id_type=MESH,
+        )
+
+    def partner_copy(j, side):
+        slot = side * same + lax.rem(place + j, same)
         return pltpu.make_async_remote_copy(
             src_ref=ntok.at[slot],
             dst_ref=ntok.at[slot],
             send_sem=f_send.at[j],
             recv_sem=t_recv.at[slot],
-            device_id=there(g, z, t + 1 - 2 * core),
+            device_id=there(g, z, partner),
             device_id_type=MESH,
         )
 
     for j in range(1, same):
-        token_copy(j).start()
-    partner_copy(0).start()
-    relays(0, third, 2 * third)
+        token_copy(j, mine).start()
+    partner_copy(0, core).start()
+    relays(third, 2 * third)
     start_own(1)
+    relays(2 * third, sp - 1)
+    for c in range(counts[0]):
+        local_copy(0, c).wait()
+
+    width = ntok.shape[2]
+
+    def up_half(side):
+        def up_step(i, _):
+            at = pl.ds(side * same + i * 2, 2)
+            x = ntok[at].reshape(2 * rows, width)
+            y = jnp.dot(x, upw[...].reshape(width, hidden_half), preferred_element_type=F32)
+            y = jnp.maximum(y, 0.0)
+            act[at] = (y * y).astype(BF16).reshape(2, rows, hidden_half)
+            return 0
+
+        lax.fori_loop(0, same // 2, up_step, 0)
+
     for j in range(1, same):
-        token_copy(j, back=True).wait_recv()
-        partner_copy(j).start()
+        token_copy(j, core * same + lax.rem(place + j, same)).wait_recv()
+        partner_copy(j, core).start()
+    up_half(core)
     for j in range(same):
-        partner_copy(j, mine=False).wait_recv()
-    relays(0, 2 * third, sp - 1)
-    for m in range(2):
-        for c in range(chunks):
-            local_copy(m, c).wait()
-
-    width = ntok.shape[2]
-    pack = 2
-
-    def up_step(i, _):
-        x = ntok[pl.ds(i * pack, pack)].reshape(pack * rows, width)
-        y = jnp.dot(x, upw[...].reshape(width, hidden_half), preferred_element_type=F32)
-        y = jnp.maximum(y, 0.0)
-        act[pl.ds(i * pack, pack)] = (y * y).astype(BF16).reshape(pack, rows, hidden_half)
+        partner_copy(j, 1 - core).wait_recv()
+    up_half(1 - core)
+    for c in range(counts[1]):
+        local_copy(1, c).wait()
+
+    pieces = counts[1]
+
+    def pre_copy(unit):
+        return pltpu.make_async_remote_copy(
+            src_ref=psend.at[unit],
+            dst_ref=precv.at[unit],
+            send_sem=p_send.at[unit],
+            recv_sem=p_recv.at[unit],
+            device_id=there(g, z, partner),
+            device_id_type=MESH,
+        )
+
+    def mlp_copy(unit, p, slot):
+        return pltpu.make_async_remote_copy(
+            src_ref=msend.at[unit, p],
+            dst_ref=mrecv.at[unit, slot],
+            send_sem=m_send.at[unit, p],
+            recv_sem=m_recv.at[unit, slot],
+            device_id=there(p // half, z, 2 * (p % half) + core),
+            device_id_type=MESH,
+        )
+
+    def down_piece(origin, c):
+        unit = origin * pieces + c
+
+        def product(side):
+            x = act[pl.ds(side * same, same)].reshape(same * rows, hidden_half)
+            return jnp.dot(x, dnw[origin, c], preferred_element_type=F32)
+
+        psend[unit] = product(1 - core).astype(BF16).reshape(psend.shape[1:])
+        pre_copy(unit).start()
+        own = product(core).reshape(psend.shape[1:])
+        pre_copy(unit).wait_recv()
+        msend[unit] = (own + precv[unit].astype(F32)).astype(BF16)
+        for p in range(same):
+            @pl.when(p != place)
+            def _():
+                mlp_copy(unit, p, place).start()
+
+    for c in range(pieces):
+        down_piece(z, c)
+
+    def down_step(s, _):
+        for c in range(pieces):
+            relay(1, s, c)
+
+            @pl.when(z - 1 - s >= 0)
+            def _():
+                down_piece(z - 1 - s, c)
+
+            @pl.when(z + 1 + s < sp)
+            def _():
+                down_piece(z + 1 + s, c)
+
         return 0
 
-    lax.fori_loop(0, layer // pack, up_step, 0)
-
-    out_cols = down_ref.shape[1]
-
-    def mlp_copy(origin, j):
-        d = lax.rem(me + j, layer)
-        return pltpu.make_async_remote_copy(
-            src_ref=msend.at[origin, j],
-            dst_ref=mrecv.at[origin, j],
-            send_sem=m_send.at[origin, j],
-            recv_sem=m_recv.at[origin, j],
-            device_id=there(d // tp, z, lax.rem(d, tp)),
-            device_id_type=MESH,
-        )
-
-    def down_piece(origin):
-        w = dnw[origin].reshape(hidden_half, out_cols)
-
-        def step(i, _):
-            j = layer - 1 - i
-            x = act[lax.rem(me + j, layer)]
-            msend[origin, j] = jnp.dot(x, w, preferred_element_type=F32).astype(BF16)
-
-            @pl.when(j > 0)
-            def _():
-                mlp_copy(origin, j).start()
-
-            return 0
-
-        lax.fori_loop(0, layer, step, 0)
-
-    down_piece(z)
-
-    def down_step(s, _):
-        relay(1, s)
-
-        @pl.when(z - 1 - s >= 0)
-        def _():
-            down_piece(z - 1 - s)
-
-        @pl.when(z + 1 + s < sp)
-        def _():
-            down_piece(z + 1 + s)
+    lax.fori_loop(0, sp - 1, down_step, 0)
+
+    def finish_unit(origin, c):
+        unit = origin * pieces + c
+        mrecv[unit, place] = msend[unit, place]
+        total = jnp.zeros(mrecv.shape[2:], F32)
+        for p in range(same):
+            @pl.when(p != place)
+            def _():
+                mlp_copy(unit, p, p).wait_recv()
+
+            total = total + mrecv[unit, p].astype(F32)
+        n = mrecv.shape[3]
+        mlp_ref[origin, :, c * n : (c + 1) * n] = total
+
+    def finish_pair(s, _):
+        @pl.when(z - s >= 0)
+        def _():
+            for c in range(pieces):
+                finish_unit(z - s, c)
+
+        @pl.when((s > 0) & (z + s < sp))
+        def _():
+            for c in range(pieces):
+                finish_unit(z + s, c)
 
         return 0
 
-    lax.fori_loop(0, sp - 1, down_step, 0)
-
-    def finish(origin, _):
-        total = msend[origin, 0].astype(F32)
-        for j in range(1, layer):
-            mlp_copy(origin, j).wait_recv()
-            total = total + mrecv[origin, j].astype(F32)
-        mlp_ref[origin] = total
-        return 0
-
-    lax.fori_loop(0, sp, finish, 0)
+    lax.fori_loop(0, sp, finish_pair, 0)
 
     def drain(origin, _):
-        for j in range(1, layer):
-            mlp_copy(origin, j).wait_send()
+        for c in range(pieces):
+            unit = origin * pieces + c
+            pre_copy(unit).wait_send()
+            for p in range(same):
+                @pl.when(p != place)
+                def _():
+                    mlp_copy(unit, p, place).wait_send()
         for m in range(2):
-            for c in range(chunks):
+            for c in range(counts[m]):
                 @pl.when((origin <= z) & (z < sp - 1))
                 def _():
                     weight_copy(m, c, origin, 0).wait_send()
@@ -389,12 +451,17 @@
         return 0
 
     lax.fori_loop(0, sp, drain, 0)
-    for j in range(1, tp):
-        branch_copy(j).wait_send()
+    for q in range(half):
+        cross_copy(q).wait_send()
+
+        @pl.when(q != pair)
+        def _():
+            branch_copy(q, pair).wait_send()
+
     for j in range(1, same):
-        token_copy(j).wait_send()
+        token_copy(j, mine).wait_send()
     for j in range(same):
-        partner_copy(j).wait_send()
+        partner_copy(j, core).wait_send()
 
     @pl.when(z < sp - 1)
     def _():
@@ -418,6 +485,10 @@
     hidden_half = hidden // grp
     out_cols = feedforward_down_matrix.shape[1]
     chunks = 2
+    pieces = 2 if out_cols % 256 == 0 else 1
+    half = tp // 2
+    same = grp * half
+    units = sp * pieces
 
     log_forget = jax.nn.log_sigmoid(forget_preactivation) + extra_forget_terms
     cum = jnp.cumsum(log_forget.reshape(heads, blocks, BLOCK), axis=-1)
@@ -439,13 +510,17 @@
         out_specs=(vmem, vmem),
         scratch_shapes=[
             pltpu.VMEM((sp, chunks, up_rows // chunks, hidden_half), BF16),
-            pltpu.VMEM((sp, chunks, hidden_half // chunks, out_cols), BF16),
+            pltpu.VMEM((sp, pieces, hidden_half, out_cols // pieces), BF16),
             pltpu.VMEM((layer, rows, width), BF16),
             pltpu.VMEM((layer, rows, hidden_half), BF16),
-            pltpu.VMEM((sp, layer, rows, out_cols), BF16),
-            pltpu.VMEM((sp, layer, rows, out_cols), BF16),
-            pltpu.VMEM((tp, rows, width), BF16),
-            pltpu.VMEM((tp, rows, width), BF16),
+            pltpu.VMEM((units, same, rows, out_cols // pieces), BF16),
+            pltpu.VMEM((units, same, rows, out_cols // pieces), BF16),
+            pltpu.VMEM((units, same, rows, out_cols // pieces), BF16),
+            pltpu.VMEM((units, same, rows, out_cols // pieces), BF16),
+            pltpu.VMEM((half, rows, width), BF16),
+            pltpu.VMEM((half, rows, width), BF16),
+            pltpu.VMEM((half, rows, width), BF16),
+            pltpu.VMEM((half, rows, width), BF16),
             pltpu.VMEM((tokens, heads * dh), BF16),
             pltpu.VMEM((heads, blocks, dh, dh), F32),
             pltpu.VMEM((heads, dh + 16, dh), F32),
@@ -455,13 +530,17 @@
             dma((2, chunks)),
             dma,
             dma,
-            dma((tp,)),
-            dma((tp,)),
+            dma((half,)),
+            dma((half,)),
+            dma((half,)),
+            dma((half,)),
+            dma((same,)),
             dma((layer,)),
-            dma((layer,)),
-            dma((layer,)),
-            dma((sp, layer)),
-            dma((sp, layer)),
+            dma((same,)),
+            dma((units,)),
+            dma((units,)),
+            dma((units, same)),
+            dma((units, same)),
         ],
         compiler_params=pltpu.CompilerParams(
             collective_id=0, has_side_effects=True, vmem_limit_bytes=60 * 1024 * 1024

time: 176 us -> 168 us (0.955)
  Pallas kernels: 168 us -> 160 us
    pallas_call x1, Pallas kernels: 168 us -> 160 us  [shards(): pl.pallas_call(functools.partial(kernel, (grp, sp, tp, heads, blocks, row...]
where the time goes in v2:
time: 168 us; the launch traced here: 167 us
  Pallas kernels  160 us (95%)
  local copies, waits for them, and re-layouts  3.65 us (2%)
  other arithmetic  3.57 us (2%)
    pallas_call x1, Pallas kernels, shards(): pl.pallas_call(functools.partial(kernel, (grp, sp, tp, heads, blocks, row...  160 us

profile of v2, /device:TPU:24, one launch (start us, length us, event | category | flops | bytes accessed | tf_op | source)
XLA Modules:
  0.0 167.0 jit_solution(6425469951519292984)
XLA Ops:
  0.0 0.7 fusion.1
  0.7 0.6 reduce_window_sum.15
  1.4 0.7 reshape.21
  2.1 0.6 sub.7.arow_ref
  2.7 0.1 copy.16
  2.8 0.0 copy-start
  2.8 0.9 copy.17
  3.7 0.7 bitcast_subtract_fusion
  4.4 0.0 copy-done
  4.4 159.7 %shard_map.127 = (bf16[128,2048]{1,0:T(8,128)(2,1)}, f32[4,128,512]{2,1,0:T(8,128)}) custom-call(bf16[512,256]{1,0:T(8,128)(2,1)} %q_ref.1, bf16[512,256]{1,0:T(8,128)(2,1)} %k_ref.1, bf16[512,256]{1,0:T(8,128)(2,1)} %v_ref.1, bf16[512,256]{1,0:T(8,128)(2,1)} %o_ref.1, f32[8,128]{1,0:T(8,128)} %sub.7.arow_ref, f32[512,2]{1,0:T(8,128)} %bitcast.12, ...), custom_call_target="tpu_custom_call" | custom-call | tf_op jit(solution)/shard_map/pallas_call | solution.py:503
  164.1 0.0 copy-start.1
  164.1 1.6 copy.18
  165.7 0.3 copy.19
  166.1 0.0 copy-done.1
  166.1 0.9 add_convert_fusion
  (1 shorter events, 0.0 us)
Async XLA Ops:
  2.8 1.6 copy-start
  164.1 2.0 %copy-start.1 = (bf16[128,2048]{1,0:T(8,128)(2,1)S(1)}, bf16[128,2048]{1,0:T(8,128)(2,1)}, u32[]{:S(2)}) copy-start(bf16[128,2048]{1,0:T(8,128)(2,1)} %get-tuple-element.7) | copy-start | bytes 1572868

commit v3 on v2

--- a/solution.py
+++ b/solution.py
@@ -99,15 +99,15 @@
     def local_copy(m, c):
         return pltpu.make_async_copy(own_piece(m, c), bufs[m].at[z, c], loc_sem.at[m, c])
 
-    def start_own(m):
-        for c in range(counts[m]):
-            @pl.when(z < sp - 1)
-            def _():
-                weight_copy(m, c, z, 0, own_piece(m, c)).start()
-
-            @pl.when(z > 0)
-            def _():
-                weight_copy(m, c, z, 1, own_piece(m, c)).start()
+    def start_right(m, c):
+        @pl.when(z < sp - 1)
+        def _():
+            weight_copy(m, c, z, 0, own_piece(m, c)).start()
+
+    def start_left(m, c):
+        @pl.when(z > 0)
+        def _():
+            weight_copy(m, c, z, 1, own_piece(m, c)).start()
 
     def relay(m, s, c):
         left, right = z - 1 - s, z + 1 + s
@@ -136,7 +136,16 @@
 
         lax.fori_loop(first, last, body, 0)
 
-    start_own(0)
+    start_right(0, 0)
+
+    @pl.when(z > 1)
+    def _():
+        for c in range(1, counts[0]):
+            start_right(0, c)
+
+    for m in range(2):
+        for c in range(counts[m]):
+            start_left(m, c)
     for m in range(2):
         for c in range(counts[m]):
             local_copy(m, c).start()
@@ -202,6 +211,14 @@
             )
             st_out[h, dh : dh + 8, :] = jnp.broadcast_to(new, (8, dh))
         state_copy().start()
+
+    @pl.when(z <= 1)
+    def _():
+        for c in range(1, counts[0]):
+            start_right(0, c)
+
+    for c in range(counts[1]):
+        start_right(1, c)
 
     third = (sp - 1) // 3
     relays(0, third)
@@ -317,8 +334,6 @@
         token_copy(j, mine).start()
     partner_copy(0, core).start()
     relays(third, 2 * third)
-    start_own(1)
-    relays(2 * third, sp - 1)
     for c in range(counts[0]):
         local_copy(0, c).wait()
 
@@ -338,6 +353,9 @@
     for j in range(1, same):
         token_copy(j, core * same + lax.rem(place + j, same)).wait_recv()
         partner_copy(j, core).start()
+    relays(2 * third, sp - 1)
+    for c in range(counts[1]):
+        relay(1, 0, c)
     up_half(core)
     for j in range(same):
         partner_copy(j, 1 - core).wait_recv()
@@ -389,7 +407,9 @@
 
     def down_step(s, _):
         for c in range(pieces):
-            relay(1, s, c)
+            @pl.when(s > 0)
+            def _():
+                relay(1, s, c)
 
             @pl.when(z - 1 - s >= 0)
             def _():

time: 168 us -> 161 us (0.958)
  Pallas kernels: 160 us -> 153 us
    pallas_call x1, Pallas kernels: 160 us -> 153 us  [shards(): pl.pallas_call(functools.partial(kernel, (grp, sp, tp, heads, blocks, row...]
where the time goes in v3:
time: 161 us; the launch traced here: 160 us
  Pallas kernels  153 us (95%)
  local copies, waits for them, and re-layouts  3.65 us (2%)
  other arithmetic  3.57 us (2%)
    pallas_call x1, Pallas kernels, shards(): pl.pallas_call(functools.partial(kernel, (grp, sp, tp, heads, blocks, row...  153 us

profile of v3, /device:TPU:24, one launch (start us, length us, event | category | flops | bytes accessed | tf_op | source)
XLA Modules:
  0.0 160.2 jit_solution(13003138478368743041)
XLA Ops:
  0.0 0.7 fusion.1
  0.7 0.6 reduce_window_sum.15
  1.4 0.7 reshape.21
  2.1 0.6 sub.7.arow_ref
  2.7 0.1 copy.16
  2.8 0.0 copy-start
  2.8 0.9 copy.17
  3.7 0.7 bitcast_subtract_fusion
  4.4 0.0 copy-done
  4.4 152.9 %shard_map.127 = (bf16[128,2048]{1,0:T(8,128)(2,1)}, f32[4,128,512]{2,1,0:T(8,128)}) custom-call(bf16[512,256]{1,0:T(8,128)(2,1)} %q_ref.1, bf16[512,256]{1,0:T(8,128)(2,1)} %k_ref.1, bf16[512,256]{1,0:T(8,128)(2,1)} %v_ref.1, bf16[512,256]{1,0:T(8,128)(2,1)} %o_ref.1, f32[8,128]{1,0:T(8,128)} %sub.7.arow_ref, f32[512,2]{1,0:T(8,128)} %bitcast.12, ...), custom_call_target="tpu_custom_call" | custom-call | tf_op jit(solution)/shard_map/pallas_call | solution.py:523
  157.3 0.0 copy-start.1
  157.3 1.6 %copy.18 = f32[128,4,512]{0,2,1:T(8,128)S(1)} copy(f32[128,4,512]{2,0,1:T(8,128)} %bitcast.13) | data formatting | bytes 2097152 | tf_op jit(solution)/shard_map/transpose | solution.py:573
  158.9 0.3 copy.19
  159.3 0.0 copy-done.1
  159.3 0.9 add_convert_fusion
  (1 shorter events, 0.0 us)
Async XLA Ops:
  2.8 1.6 %copy-start = (f32[2,4,128]{0,2,1:T(8,128)}, f32[2,4,128]{0,2,1:T(8,128)S(1)}, u32[]{:S(2)}) copy-start(f32[2,4,128]{0,2,1:T(8,128)S(1)} %copy.16) | copy-start | bytes 12292
  157.3 2.0 %copy-start.1 = (bf16[128,2048]{1,0:T(8,128)(2,1)S(1)}, bf16[128,2048]{1,0:T(8,128)(2,1)}, u32[]{:S(2)}) copy-start(bf16[128,2048]{1,0:T(8,128)(2,1)} %get-tuple-element.7) | copy-start | bytes 1572868
